TPU v7x, 128 devices: a whole 4x4x4 slice. The times are simulated.
128 devices in a mesh: sp: 32 (over z, y, core), tp: 4 (over x).
Axes of the slice: x: 4, y: 4, z: 4, core: 2. Of those that a mesh axis runs over, the one named last changes fastest.
Arguments:
- residual: bfloat16 [32768, 2048], P('sp'), may hold values from -8 to 8
- query_wide: bfloat16 [32768, 1024], P('sp', 'tp'), may hold values from -6 to 6
- key_wide: bfloat16 [32768, 1024], P('sp', 'tp'), may hold values from -6 to 6
- value_wide: bfloat16 [32768, 2048], P('sp', 'tp'), may hold values from -6 to 6
- decay_wide: bfloat16 [32768, 1024], P('sp', 'tp'), may hold values from -12 to 12
- gate_wide: bfloat16 [32768, 2048], P('sp', 'tp'), may hold values from -6 to 6
- query_narrow: bfloat16 [32768, 512], P('sp', 'tp'), may hold values from -6 to 6
- key_narrow: bfloat16 [32768, 512], P('sp', 'tp'), may hold values from -6 to 6
- value_narrow: bfloat16 [32768, 2048], P('sp', 'tp'), may hold values from -6 to 6
- decay_narrow: bfloat16 [32768, 512], P('sp', 'tp'), may hold values from -12 to 12
- gate_narrow: bfloat16 [32768, 2048], P('sp', 'tp'), may hold values from -6 to 6
- head_gain: float32 [512], replicated, may hold values from 0.1 to 1.9
- out_wide: bfloat16 [2048, 2048], P('tp'), may hold values from -0.125 to 0.125
- out_narrow: bfloat16 [2048, 2048], P('tp'), may hold values from -0.125 to 0.125
- mlp_gain: float32 [2048], replicated, may hold values from 0.1 to 1.9
- up_weight: bfloat16 [2048, 4096], P('sp', 'tp'), may hold values from -0.125 to 0.125
- down_weight: bfloat16 [4096, 2048], P('tp', 'sp'), may hold values from -0.09375 to 0.09375
Outputs:
- layer_out: bfloat16 [32768, 2048], P('sp', 'tp')
All inputs are finite; a program needn't handle non-finite values.
Results may differ from a plain program's by a relative error of at most 0.017.
Values may be sent and summed in bfloat16 or wider, within the bound.
A program may use at most 128 MiB of HBM per device.

v0:
```python
import jax
import jax.numpy as jnp
from jax import lax
from jax.sharding import PartitionSpec as P

HEADS = 4
BLOCK = 64


EPS = 1e-05
DECAY_NORMALIZER = 16.0
HIGHEST = lax.Precision.HIGHEST


def turned_gather(arrays, axis, dims):
    turned = [jnp.moveaxis(a, dim, 0) for a, dim in zip(arrays, dims)]
    both = jnp.concatenate([t.reshape(len(t), -1) for t in turned], axis=1)
    whole, at, finished = (lax.all_gather(both, axis, axis=0, tiled=True), 0, [])
    for t, dim in zip(turned, dims):
        section = whole[:, at : at + t[0].size].reshape(-1, *t.shape[1:])
        finished.append(jnp.moveaxis(section, 0, dim))
        at += t[0].size
    return tuple(finished)


def entering(array, axis, join, neutral):
    place = lax.axis_index(axis)
    gathered = jax.tree.map(
        lambda a, kind: lax.all_gather(a.astype(kind), axis),
        array,
        (jnp.bfloat16, jnp.bfloat16, jnp.bfloat16, jnp.bfloat16),
    )
    state = jax.tree.map(lambda a, e: jnp.zeros_like(a) + jnp.asarray(e, a.dtype), array, neutral)

    def one(step, state):
        return join(
            state,
            jax.tree.map(
                lambda a, own: lax.dynamic_index_in_dim(a, step, 0, False).astype(own.dtype),
                gathered,
                array,
            ),
        )

    return lax.fori_loop(0, place, one, state)


def split_up(array, dim, count):
    dims = array.shape
    pieces = array.reshape(*dims[:dim], count, dims[dim] // count, *dims[dim + 1 :])
    return jnp.moveaxis(pieces, dim, 0)


def sum_at_owner(array, axis, dim):
    count = lax.axis_size(axis)
    pieces = lax.all_to_all(split_up(array, dim, count), axis, 0, 0, tiled=True)
    return jnp.sum(pieces.astype(jnp.float32), axis=0)


def sent_to_all(array, axis):
    copies = jnp.broadcast_to(array, (lax.axis_size(axis), *array.shape))
    return lax.all_to_all(copies, axis, split_axis=0, concat_axis=0, tiled=True)


def of_everyone(array, axis):
    everything = sent_to_all(array, axis)
    return jnp.sum(everything, axis=0)


def block_pass(queries, keys_in, values_in, log_decay, block_len):
    num_blocks = queries.shape[0] // block_len

    def to_blocks(stacked):
        return stacked.reshape((num_blocks, block_len) + stacked.shape[1:])

    causal = jnp.tril(jnp.ones((block_len, block_len), dtype=bool))
    initial = (
        jnp.zeros((queries.shape[1], queries.shape[2], values_in.shape[2]), jnp.float32),
        jnp.zeros((queries.shape[1], queries.shape[2]), jnp.float32),
    )

    def advance(running, inputs):
        memory, offset = running
        block_q, block_k, block_v, block_g = inputs
        within = jnp.cumsum(block_g, axis=0)
        final_log = within[-1]
        scaled_q = block_q * jnp.exp(within)
        scaled_k = block_k * jnp.exp(-within)
        outside = jnp.einsum("ihd,hde->ihe", scaled_q, memory, precision=HIGHEST)
        scores = jnp.einsum("ihd,jhd->hij", scaled_q, scaled_k, precision=HIGHEST)
        scores = jnp.where(causal[None], scores, 0.0)
        inside = jnp.einsum("hij,jhe->ihe", scores, block_v, precision=HIGHEST)
        decayed_keys = scaled_k * jnp.exp(final_log)[None]
        memory = jnp.exp(final_log)[..., None] * memory + jnp.einsum(
            "jhd,jhe->hde", decayed_keys, block_v, precision=HIGHEST
        )
        carried_q = scaled_q * jnp.exp(offset)[None]
        return ((memory, offset + final_log), (outside + inside, carried_q))

    (memory, totals), (outputs, carried_q) = lax.scan(
        advance,
        initial,
        (to_blocks(queries), to_blocks(keys_in), to_blocks(values_in), to_blocks(log_decay)),
    )
    return (outputs.reshape(values_in.shape), carried_q.reshape(queries.shape), totals, memory)


def prepare(query, key_proj, value, decay, heads_here):
    row_count = query.shape[0]
    key_width = query.shape[1] // heads_here
    queries = query.astype(jnp.float32).reshape(row_count, heads_here, key_width) * key_width ** (
        -0.5
    )
    keys_in = key_proj.astype(jnp.float32).reshape(row_count, heads_here, key_width)
    values_in = value.astype(jnp.float32).reshape(
        row_count, heads_here, value.shape[1] // heads_here
    )
    log_decay = (
        jax.nn.log_sigmoid(decay.astype(jnp.float32)).reshape(row_count, heads_here, key_width)
        / DECAY_NORMALIZER
    )
    return (queries, keys_in, values_in, log_decay)


def finish(outputs, gate, head_gain):
    scale = lax.rsqrt(jnp.mean(jnp.square(outputs), axis=-1, keepdims=True) + EPS)
    gated = (
        outputs * scale * head_gain * jax.nn.silu(gate.astype(jnp.float32).reshape(outputs.shape))
    )
    return gated.reshape(outputs.shape[0], -1).astype(jnp.bfloat16)


def combine_states(earlier, later):
    return (
        earlier[0] + later[0],
        jnp.exp(later[0])[..., None] * earlier[1] + later[1],
        earlier[2] + later[2],
        jnp.exp(later[2])[..., None] * earlier[3] + later[3],
    )


def body(
    residual,
    query_wide,
    key_wide,
    value_wide,
    decay_wide,
    gate_wide,
    query_narrow,
    key_narrow,
    value_narrow,
    decay_narrow,
    gate_narrow,
    head_gain,
    out_wide,
    out_narrow,
    mlp_gain,
    up_weight,
    down_weight,
):
    heads_here = HEADS // lax.axis_size("tp")
    up_whole, down_whole = turned_gather((up_weight, down_weight), "sp", (0, 1))
    wq, wk, wv, wg = prepare(query_wide, key_wide, value_wide, decay_wide, heads_here)
    wide_out, wide_q, wide_total, wide_memory = block_pass(wq, wk, wv, wg, BLOCK)
    nq, nk, nv, ng = prepare(query_narrow, key_narrow, value_narrow, decay_narrow, heads_here)
    narrow_out, narrow_q, narrow_total, narrow_memory = block_pass(nq, nk, nv, ng, BLOCK)
    identity = (
        jnp.zeros_like(wide_total),
        jnp.zeros_like(wide_memory),
        jnp.zeros_like(narrow_total),
        jnp.zeros_like(narrow_memory),
    )
    incoming = entering(
        (wide_total, wide_memory, narrow_total, narrow_memory), "sp", combine_states, identity
    )
    wide_out = wide_out + jnp.einsum("ihd,hde->ihe", wide_q, incoming[1], precision=HIGHEST)
    narrow_out = narrow_out + jnp.einsum("ihd,hde->ihe", narrow_q, incoming[3], precision=HIGHEST)
    gated_wide = finish(wide_out, gate_wide, head_gain)
    gated_narrow = finish(narrow_out, gate_narrow, head_gain)
    head_terms = jnp.dot(gated_wide, out_wide, preferred_element_type=jnp.float32) + jnp.dot(
        gated_narrow, out_narrow, preferred_element_type=jnp.float32
    )
    tp_index = lax.axis_index("tp")
    col_count = residual.shape[1] // lax.axis_size("tp")
    full_width = residual.shape[1]
    residual_cols = lax.dynamic_slice_in_dim(residual, tp_index * col_count, col_count, 1)
    mixed_cols = sum_at_owner(head_terms.astype(jnp.bfloat16), "tp", 1)
    stream_cols = (residual_cols.astype(jnp.float32) + mixed_cols).astype(jnp.bfloat16)
    stream_f = stream_cols.astype(jnp.float32)
    squares = of_everyone(jnp.sum(jnp.square(stream_f), axis=1, keepdims=True), "tp")
    gain_cols = lax.dynamic_slice_in_dim(mlp_gain, tp_index * col_count, col_count, 0)
    normed_cols = (stream_f * lax.rsqrt(squares / full_width + EPS) * gain_cols).astype(
        jnp.bfloat16
    )
    normed = lax.all_gather(normed_cols, "tp", axis=1, tiled=True)
    before_activation = jnp.dot(normed, up_whole, preferred_element_type=jnp.float32)
    hidden = jnp.square(jax.nn.relu(before_activation)).astype(jnp.bfloat16)
    down_terms = jnp.dot(hidden, down_whole, preferred_element_type=jnp.float32)
    mlp_cols = sum_at_owner(down_terms.astype(jnp.bfloat16), "tp", 1)
    return (stream_cols.astype(jnp.float32) + mlp_cols).astype(jnp.bfloat16)


def solution(mesh):
    return jax.shard_map(
        body,
        mesh=mesh,
        in_specs=(
            P("sp", None),
            P("sp", "tp"),
            P("sp", "tp"),
            P("sp", "tp"),
            P("sp", "tp"),
            P("sp", "tp"),
            P("sp", "tp"),
            P("sp", "tp"),
            P("sp", "tp"),
            P("sp", "tp"),
            P("sp", "tp"),
            P(),
            P("tp", None),
            P("tp", None),
            P(),
            P("sp", "tp"),
            P("tp", "sp"),
        ),
        out_specs=P("sp", "tp"),
        check_vma=False,
    )
```

profile of v0, /device:TPU:0, one launch (start us, length us, event | category | flops | bytes accessed | tf_op | source)
XLA Modules:
  0.0 539.1 jit_solution(10759921777863404328)
XLA Ops:
  6.6 5.0 reshape.518
  11.7 1.1 fusion.98
  13.8 1.7 broadcast.136.clone.1
  15.4 68.4 %while.51 = (s32[]{:T(128)}, f32[1,128,512]{2,1,0:T(8,128)S(1)}, f32[1,128]{1,0:T(1,128)S(1)}, f32[16,64,1,512]{3,1,2,0:T(8,128)}, f32[16,64,1,128]{3,1,2,0:T(8,...) while((s32[]{:T(128)}, f32[1,128,512]{2,1,0:T(8,128)S(1)}, ...), condition=%wide.region_5.6_spmd.clone, body=%wide.region_3.5_spmd.clone.sunk | while | flops 133005568 | bytes 2333321 | solution.py:100
  84.7 2.7 fusion.90
  87.3 3.3 reshape.501
  91.6 3.4 reshape.502
  95.0 4.9 reshape.516
  99.8 2.0 reshape.515
  101.9 1.6 broadcast.136.clone
  103.5 108.8 %while.50 = (s32[]{:T(128)}, f32[1,256,512]{2,1,0:T(8,128)S(1)}, f32[1,256]{1,0:T(1,128)S(1)}, f32[16,64,1,512]{3,1,2,0:T(8,128)}, f32[16,64,1,256]{3,1,2,0:T(8,...) while((s32[]{:T(128)}, f32[1,256,512]{2,1,0:T(8,128)S(1)}, ...), condition=%wide.region_2.3_spmd.clone, body=%wide.region_0.2_spmd.clone.sunk | while | flops 240787968 | bytes 3648133 | solution.py:100
  104.5 1.1 broadcast_multiply_fusion.2
  107.0 1.1 fusion.158
  111.3 1.1 broadcast_multiply_fusion.2
  113.7 1.1 fusion.158
  118.1 1.1 broadcast_multiply_fusion.2
  120.5 1.1 fusion.158
  124.9 1.1 broadcast_multiply_fusion.2
  127.4 1.1 fusion.158
  131.7 1.1 broadcast_multiply_fusion.2
  134.2 1.1 fusion.158
  138.5 1.1 broadcast_multiply_fusion.2
  141.0 1.1 fusion.158
  145.3 1.1 broadcast_multiply_fusion.2
  147.8 1.1 fusion.158
  152.1 1.1 broadcast_multiply_fusion.2
  154.6 1.1 fusion.158
  158.9 1.1 broadcast_multiply_fusion.2
  161.3 1.1 fusion.158
  165.7 1.1 broadcast_multiply_fusion.2
  168.1 1.1 fusion.158
  172.4 1.1 broadcast_multiply_fusion.2
  174.9 1.1 fusion.158
  181.7 1.1 fusion.158
  186.0 1.1 broadcast_multiply_fusion.2
  188.5 1.1 fusion.158
  192.8 1.1 broadcast_multiply_fusion.2
  195.3 1.1 fusion.158
  199.7 1.1 broadcast_multiply_fusion.2
  202.1 1.1 fusion.158
  208.9 1.1 fusion.158
  213.9 3.0 copy.32
  216.9 1.3 copy.33
  218.2 3.0 copy.34
  221.3 1.4 copy.35
  222.6 23.1 %all-gather.5 = bf16[32,1,128]{2,1,0:T(2,128)(2,1)S(1)} all-gather(bf16[1,1,128]{2,1,0:T(2,128)(2,1)S(1)} %convert_bitcast_fusion.1), channel_id=4, replica_groups=mesh['sp'=32,'tp'=4] {'sp'}, dimensions={0}, use_global_device_ids=true | all-gather | bytes 8448 | tf_op jit(solution)/shard_map/all_gather | solution.py:29
  245.7 23.8 %all-gather.4 = bf16[32,1,256]{2,1,0:T(2,128)(2,1)S(1)} all-gather(bf16[1,1,256]{2,1,0:T(2,128)(2,1)S(1)} %convert_bitcast_fusion), channel_id=2, replica_groups=mesh['sp'=32,'tp'=4] {'sp'}, dimensions={0}, use_global_device_ids=true | all-gather | bytes 16896 | tf_op jit(solution)/shard_map/all_gather | solution.py:29
  269.6 5.6 %multiply_reduce_fusion.1 = (f32[1024]{0:T(1024)S(1)}, f32[1024,1,512]{0,2,1:T(8,128)S(1)}) fusion(f32[1024,1,512]{0,2,1:T(8,128)} %copy.32, f32[1024,256]{1,0:T(8,128)} %bitcast.301, f32[1,256,512]{2,1,0:T(8,128)S(1)} %get-tuple-element.190), kind=kOutput, calls=%fused_computation.128 | convolution fusion | flops 1612184576 | bytes 5771264 | tf_op jit(solution)/shard_map/ihd,hde->ihe/dot_general | solution.py:176
  275.3 2.0 multiply_reduce_fusion
  277.4 2.8 fusion.87
  280.2 3.1 add_convert_fusion
  283.3 2.2 copy.90
  285.5 5.1 all-to-all-start
  290.7 48.5 %all-to-all-done = bf16[4,1024,512]{2,1,0:T(8,128)(2,1)} async-done(((bf16[4,1024,512]{2,1,0:T(8,128)(2,1)}), bf16[4,1024,512]{2,1,0:T(8,128)(2,1)}, u32[]{:S(2)}, u32[]{:S(2)}) %all-to-all-start) | async-done | bytes 4194336 | tf_op jit(solution)/shard_map/all_to_all | solution.py:56
  339.1 3.0 convert_reduce_fusion.1
  342.2 1.6 fusion.80
  344.4 3.3 all-to-all-start.1
  348.5 4.5 all-to-all-done.1
  353.0 1.3 fusion.82
  354.4 111.0 %all-gather.11.cloned.1.call-done = bf16[1024,2048]{1,0:T(8,128)(2,1)} async-done(((bf16[1024,512]{1,0:T(8,128)(2,1)}), bf16[1024,2048]{1,0:T(8,128)(2,1)}) %all-gather.11.cloned.1.call-update) | async-done | bytes 4194320 | tf_op jit(solution)/shard_map/all_gather | solution.py:195
  465.4 8.1 %multiply_convert_fusion = bf16[1024,1024]{1,0:T(8,128)(2,1)S(1)} fusion(bf16[1024,2048]{1,0:T(8,128)(2,1)} %all-gather.11.cloned.1.call-done, bf16[2048,2048]{1,0:T(8,128)(2,1)} %all-gather.13.cloned.1.call-done), kind=kOutput, calls=%fused_computation.98 | convolution fusion | flops 4298113024 | bytes 10485760 | tf_op jit(solution)/shard_map/dot_general | solution.py:196
  473.5 4.8 fusion.63
  478.7 51.8 %all_to_all.15 = bf16[4,1024,512]{2,1,0:T(8,128)(2,1)S(1)} all-to-all(bf16[4,1024,512]{2,1,0:T(8,128)(2,1)S(1)} %bitcast.288), channel_id=1, replica_groups=mesh['sp'=32,'tp'=4] {'tp'}, dimensions={0} | all-to-all | bytes 8388608 | tf_op jit(solution)/shard_map/all_to_all | solution.py:56
  531.1 1.4 fusion.83
  (392 shorter events, 150.0 us)
Async XLA Ops:
  6.5 270.8 %copy-start = (bf16[512,2048]{1,0:T(8,128)(2,1)S(1)}, bf16[512,2048]{1,0:T(8,128)(2,1)}, u32[]{:S(2)}) copy-start(bf16[512,2048]{1,0:T(8,128)(2,1)} %param.35) | copy-start | bytes 6291460
  6.5 5.1 copy-start.10
  6.5 5.1 copy-start.11
  6.5 263.0 %all-gather.17.cloned.1.call-start = ((), (), s32[]{:S(2)}) async-start(), calls=%async_computation.6 | async-start | bytes 4325376 | tf_op jit(solution)/shard_map/all_gather | solution.py:29
  83.9 6.7 %copy-start.7 = (bf16[1024,256]{1,0:T(8,128)(2,1)S(1)}, bf16[1024,256]{1,0:T(8,128)(2,1)}, u32[]{:S(2)}) copy-start(bf16[1024,256]{1,0:T(8,128)(2,1)} %param.24) | copy-start | bytes 1572868
  84.6 184.9 %all-gather.15.cloned.1.call-start = ((), (), s32[]{:S(2)}) async-start(), calls=%async_computation.5 | async-start | bytes 8650752 | tf_op jit(solution)/shard_map/all_gather | solution.py:29
  91.6 8.2 %copy-start.8 = (bf16[1024,256]{1,0:T(8,128)(2,1)S(1)}, bf16[1024,256]{1,0:T(8,128)(2,1)}, u32[]{:S(2)}) copy-start(bf16[1024,256]{1,0:T(8,128)(2,1)} %param.25) | copy-start | bytes 1572868
  103.5 109.6 %copy-start.12 = (bf16[1024,64]{0,1:T(8,128)(2,1)S(1)}, bf16[1024,64]{0,1:T(8,128)(2,1)}, u32[]{:S(2)}) copy-start(bf16[1024,64]{0,1:T(8,128)(2,1)} %param.39) | copy-start | bytes 393220
  103.5 109.6 %copy-start.13 = (bf16[64,1024]{1,0:T(8,128)(2,1)S(1)}, bf16[64,1024]{1,0:T(8,128)(2,1)}, u32[]{:S(2)}) copy-start(bf16[64,1024]{1,0:T(8,128)(2,1)} %param.38) | copy-start | bytes 393220
  213.1 141.3 %all-gather.13.cloned.1.call-start = ((), (), s32[]{:S(2)}) async-start(), calls=%async_computation.4 | async-start | bytes 8650752 | tf_op jit(solution)/shard_map/all_gather | solution.py:18
  213.9 3.0 copy-start.3
  218.2 3.0 copy-start.4
  269.6 5.7 %copy-start.2 = (f32[1024,1,512]{0,2,1:T(8,128)S(1)}, f32[1024,1,512]{0,2,1:T(8,128)}, u32[]{:S(2)}) copy-start(f32[1024,1,512]{0,2,1:T(8,128)} %copy.34) | copy-start | bytes 6291460
  269.6 5.7 %copy-start.9 = (f32[16,64,1,128]{3,1,2,0:T(8,128)S(1)}, f32[16,64,1,128]{3,1,2,0:T(8,128)}, u32[]{:S(2)}) copy-start(f32[16,64,1,128]{3,1,2,0:T(8,128)} %get-tuple-element.194) | copy-start | bytes 1572868
  275.3 2.1 copy-start.6
  275.3 2.1 copy-start.16
  277.4 2.8 copy-start.5
  277.4 2.8 copy-start.15
  285.5 53.6 %all-to-all-start = ((bf16[4,1024,512]{2,1,0:T(8,128)(2,1)}), bf16[4,1024,512]{2,1,0:T(8,128)(2,1)}, u32[]{:S(2)}, u32[]{:S(2)}) async-start(bf16[4,1024,512]{2,1,0:T(8,128)(2,1)} %bitcast.287), calls=%async_computation | async-start | bytes 8388608 | tf_op jit(solution)/shard_map/all_to_all | solution.py:56
  344.4 8.6 %all-to-all-start.1 = ((f32[4,1024,1]{1,2,0:T(1,128)}), f32[4,1024,1]{1,2,0:T(1,128)S(1)}, u32[]{:S(2)}, u32[]{:S(2)}) async-start(f32[4,1024,1]{1,2,0:T(1,128)} %broadcast_in_dim.50), calls=%async_computation.1 | async-start | bytes 32768 | tf_op jit(solution)/shard_map/all_to_all | solution.py:62
  347.7 117.7 %all-gather.11.cloned.1.call-start = ((), (), s32[]{:S(2)}) async-start(), calls=%async_computation.3 | async-start | bytes 5242880 | tf_op jit(solution)/shard_map/all_gather | solution.py:195
  465.4 8.1 %copy-start.14 = (bf16[2048,2048]{1,0:T(8,128)(2,1)S(1)}, bf16[2048,2048]{1,0:T(8,128)(2,1)}, u32[]{:S(2)}) copy-start(bf16[2048,2048]{1,0:T(8,128)(2,1)} %all-gather.13.cloned.1.call-done) | copy-start | bytes 25165828
  530.4 2.1 copy-start.1
Sparse Core Ops, SparseCore 0:
  84.7 48.7 all-gather.16
  213.2 55.4 all-gather.14
  271.0 52.3 all-gather.12
  354.5 110.8 all-gather.10
where the time goes:
time: 545 us; the launch traced here: 539 us
  waiting for transfers between devices  164 us (30%)
  blocking collectives  98.6 us (18%)
  matrix products  91.9 us (17%)
  local copies, waits for them, and re-layouts  86.4 us (16%)
  other arithmetic  74.3 us (14%)
  between operations  13.5 us (2%)
  starting transfers between devices  8.53 us (2%)
    all_gather x1, waiting for transfers between devices, body(): normed = lax.all_gather(normed_cols, 'tp', axis=1, tiled=True)  111 us
    all_to_all x1, blocking collectives, sum_at_owner(): pieces = lax.all_to_all(split_up(array, dim, count), axis, 0, 0, tiled=True)  51.8 us
    all_to_all x1, waiting for transfers between devices, sum_at_owner(): pieces = lax.all_to_all(split_up(array, dim, count), axis, 0, 0, tiled=True)  48.5 us
    all_gather x2, blocking collectives, entering(): lax.all_gather(a.astype(kind), axis)  46.9 us
    dynamic_slice x48, local copies, waits for them, and re-layouts, block_pass(): lax.scan(advance, initial, (to_blocks(queries), to_blocks(keys_in), to_bl...  41.7 us
    dot_general x32, matrix products, advance(): outside = jnp.einsum('ihd,hde->ihe', scaled_q, memory, precision=HIGHEST)  22.1 us
    dot_general x32, matrix products, advance(): inside = jnp.einsum('hij,jhe->ihe', scores, block_v, precision=HIGHEST)  19.3 us
    dot_general x32, matrix products, advance(): jnp.einsum('jhd,jhe->hde', decayed_keys, block_v, precision=HIGHEST)  17.8 us
  transfers between devices with their start and end apart: 6, of which 3 were waited for; matrix products, arithmetic and copies ran while one was open for 30% of the time, Pallas kernels for 0%

commit v1 on v0

v1 whole, which is shorter than its diff:
```python
import jax
import jax.numpy as jnp
from jax import lax
from jax.experimental import pallas as pl
from jax.experimental.pallas import tpu as pltpu
from jax.sharding import PartitionSpec as P

MESH = pl.DeviceIdType.MESH
F32, BF16 = jnp.float32, jnp.bfloat16
EPS = 1e-05
C = 128
CH = 8
KA, KB, KK = 256, 128, 384
S = 4
R = 64
D = 2048
H = 1024


def dot(a, b):
    return jnp.dot(a, b, preferred_element_type=F32)


def dot_nt(a, b):
    return lax.dot_general(a, b, (((1,), (1,)), ((), ())), preferred_element_type=F32)


def dot_tn(a, b):
    return lax.dot_general(a, b, (((0,), (0,)), ((), ())), preferred_element_type=F32)


def kernel(
    res, qw, kw, vw, dw, gw, qn, kn, vn, dn, gn, ow, on, upw, dnw, gain, mgain,
    out,
    q_s, k_s, d_s, v_s, g_s, o_s, res_s, xw, up, down, qd, qo, mc, m_s, sb, dt,
    r1, rd1, t2, dt2, r2, rd2, s3, m_in, att, px, rxa, rxb, st, xs, py, rya, ryb, hid, fin, outb,
    ld, w1s, w1r, w2s, w2r, w3s, w3r, w3fs, w3fr, w4s, w4r,
    s1s, s1r, s1ds, s1dr, s2s, s2r, s2ds, s2dr, s3s, s3r,
    xas, xar, xbs, xbr, yas, yar, ybs, ybr, ags, agr, afs, afr, oas, oar, ods,
):
    sp = lax.axis_index("sp")
    x = lax.axis_index("tp")
    core = lax.rem(sp, 2)
    y = lax.rem(lax.div(sp, 2), 4)
    z = lax.div(sp, 8)
    me = lax.rem(sp, 8)

    def at(xx, yy, zz, cc):
        return ((zz * 4 + yy) * 2 + cc, xx)

    def m4(v):
        return lax.rem(v + 8, 4)

    def remote(src, dst, ss, rs, dev):
        return pltpu.make_async_remote_copy(
            src_ref=src, dst_ref=dst, send_sem=ss, recv_sem=rs, device_id=dev, device_id_type=MESH
        )

    tok = pl.ds(pl.multiple_of(x * (S * R), S * R), S * R)
    loads = [
        (upw, xw.at[x, 0:64]),
        (dnw, xw.at[x, 64:128]),
        (dw, d_s.at[:, 0:KA]),
        (dn, d_s.at[:, KA:KK]),
        (kw, k_s.at[:, 0:KA]),
        (kn, k_s.at[:, KA:KK]),
        (qw, q_s.at[:, 0:KA]),
        (qn, q_s.at[:, KA:KK]),
        (vw, v_s.at[:, 0:512]),
        (vn, v_s.at[:, 512:1024]),
        (gw, g_s.at[:, 0:512]),
        (gn, g_s.at[:, 512:1024]),
        (ow, o_s.at[0:512]),
        (on, o_s.at[512:1024]),
        (res.at[tok], res_s),
    ]
    loads = [pltpu.make_async_copy(a, b, ld.at[i]) for i, (a, b) in enumerate(loads)]
    for c in loads:
        c.start()

    barrier = pltpu.get_barrier_semaphore()
    for d in (1, 2, 3):
        pl.semaphore_signal(barrier, inc=1, device_id=at(m4(x + d), y, z, core), device_id_type=MESH)
        pl.semaphore_signal(barrier, inc=1, device_id=at(x, y, m4(z + d), core), device_id_type=MESH)
    for d in range(1, 8):
        j = lax.rem(me + d, 8)
        pl.semaphore_signal(barrier, inc=1, device_id=(z * 8 + j, x), device_id_type=MESH)
    pl.semaphore_wait(barrier, 13)

    def w1(d):
        t = m4(x + d)
        return remote(xw.at[x], xw.at[x], w1s.at[t], w1r.at[x], at(t, y, z, core))

    loads[0].wait()
    loads[1].wait()
    for d in (1, 3, 2):
        w1(d).start()

    row_i = lax.broadcasted_iota(jnp.int32, (C, C), 0)
    col_i = lax.broadcasted_iota(jnp.int32, (C, C), 1)
    causal = col_i <= row_i
    lower = causal.astype(BF16)
    lane = lax.broadcasted_iota(jnp.int32, (1, KK), 1)
    scale = jnp.where(lane < KA, KA**-0.5, KB**-0.5).astype(F32)
    for c in loads[2:10]:
        c.wait()
    m_s[...] = jnp.zeros_like(m_s)

    def first(c, off):
        rows = pl.ds(pl.multiple_of(c * C, C), C)
        dd = d_s[rows, :].astype(F32)
        g = (jnp.minimum(dd, 0.0) - jnp.log1p(jnp.exp(-jnp.abs(dd)))) * (1.0 / 16.0)
        high = g.astype(BF16)
        low = (g - high.astype(F32)).astype(BF16)
        within = dot(lower, high) + dot(lower, low)
        mid = within[C // 2 - 1 : C // 2, :]
        last = within[C - 1 : C, :]
        qf = q_s[rows, :].astype(F32) * scale
        kf = k_s[rows, :].astype(F32)
        decayed = qf * jnp.exp(within)
        q_s[rows, :] = (qf * jnp.exp(within - mid)).astype(BF16)
        k_s[rows, :] = (kf * jnp.exp(mid - within)).astype(BF16)
        qd[rows, :] = decayed.astype(BF16)
        qo[rows, :] = (decayed * jnp.exp(off)).astype(BF16)
        kd = (kf * jnp.exp(last - within)).astype(BF16)
        mc[c] = m_s[...].astype(BF16)
        fade = jnp.exp(last)
        m_s[:, 0:KA] = m_s[:, 0:KA] * fade[:, 0:KA] + dot_tn(v_s[rows, 0:512], kd[:, 0:KA])
        m_s[:, KA:KK] = m_s[:, KA:KK] * fade[:, KA:KK] + dot_tn(v_s[rows, 512:1024], kd[:, KA:KK])
        return off + last

    total = lax.fori_loop(0, CH, first, jnp.zeros((1, KK), F32))
    sb[...] = m_s[...].astype(BF16)
    dt[...] = jnp.broadcast_to(total, (8, KK))

    def part(j):
        return pl.ds(pl.multiple_of(j * 64, 64), 64)

    def s1(d):
        j = lax.rem(me + d, 8)
        dev = (z * 8 + j, x)
        return (
            remote(sb.at[part(j)], r1.at[me], s1s.at[j], s1r.at[me], dev),
            remote(dt, rd1.at[me], s1ds.at[j], s1dr.at[me], dev),
        )

    for d in range(1, 8):
        for c in s1(d):
            c.start()
    r1[me] = sb[part(me), :]
    rd1[me] = dt[...]

    own = pl.ds(pl.multiple_of(sp * 64, 64), 64)

    def w2(d):
        q = m4(x + y + d)
        dev = at(x, m4(y + d), z, core)
        return (
            remote(xw.at[q, 0:64], up.at[own], w2s.at[0, q], w2r.at[0, y], dev),
            remote(xw.at[q, 64:128], down.at[own], w2s.at[1, q], w2r.at[1, y], dev),
        )

    def second(c, _):
        rows = pl.ds(pl.multiple_of(c * C, C), C)
        for ks, vs in ((slice(0, KA), slice(0, 512)), (slice(KA, KK), slice(512, 1024))):
            sc = dot_nt(q_s[rows, ks], k_s[rows, ks])
            sc = jnp.where(causal, sc, 0.0).astype(BF16)
            att[rows, vs] = dot(sc, v_s[rows, vs]) + dot_nt(qd[rows, ks], mc[c, :, ks])
        return 0

    lax.fori_loop(0, CH, second, 0)

    for d in range(1, 8):
        j = lax.rem(me + d, 8)
        remote(sb.at[part(me)], r1.at[j], s1s.at[j], s1r.at[j], (z * 8 + j, x)).wait_recv()
        remote(dt, rd1.at[j], s1ds.at[j], s1dr.at[j], (z * 8 + j, x)).wait_recv()

    def over_cores(j, carry):
        acc, dacc = carry
        dj = rd1[j][0:1, :]
        return acc * jnp.exp(dj) + r1[j].astype(F32), dacc + dj

    acc, dacc = lax.fori_loop(
        0, 8, over_cores, (jnp.zeros((64, KK), F32), jnp.zeros((1, KK), F32))
    )
    t2[...] = acc.astype(BF16)
    dt2[...] = jnp.broadcast_to(dacc, (8, KK))

    def s2(d):
        t = m4(z + d)
        dev = at(x, y, t, core)
        return (
            remote(t2, r2.at[z], s2s.at[t], s2r.at[z], dev),
            remote(dt2, rd2.at[z], s2ds.at[t], s2dr.at[z], dev),
        )

    for d in (1, 3, 2):
        for c in s2(d):
            c.start()
    r2[z] = t2[...]
    rd2[z] = dt2[...]
    for d in (1, 2, 3):
        t = m4(x + d)
        remote(xw.at[t], xw.at[t], w1s.at[t], w1r.at[t], at(t, y, z, core)).wait_recv()
    quarter = m4(x + y)
    up[own, :] = xw[quarter, 0:64]
    down[own, :] = xw[quarter, 64:128]
    for d in (1, 2, 3):
        t = m4(z + d)
        remote(t2, r2.at[t], s2s.at[t], s2r.at[t], at(x, y, t, core)).wait_recv()
        remote(dt2, rd2.at[t], s2ds.at[t], s2dr.at[t], at(x, y, t, core)).wait_recv()

    def over_z(t, acc):
        return jnp.where(t < z, acc * jnp.exp(rd2[t][0:1, :]) + r2[t].astype(F32), acc)

    acc = lax.fori_loop(0, 4, over_z, jnp.zeros((64, KK), F32))

    def hand_out(j, acc):
        s3[j] = acc.astype(BF16)
        return acc * jnp.exp(rd1[j][0:1, :]) + r1[j].astype(F32)

    lax.fori_loop(0, 8, hand_out, acc)

    def s3c(d):
        j = lax.rem(me + d, 8)
        return remote(s3.at[j], m_in.at[part(me)], s3s.at[j], s3r.at[me], (z * 8 + j, x))

    for d in range(1, 8):
        s3c(d).start()
    m_in[part(me), :] = s3[me]

    for d in (1, 3, 2):
        for c in w2(d):
            c.start()

    def piece(zz, p):
        return pl.ds(pl.multiple_of(((zz * 4 + p) * 2 + core) * 64, 64), 64)

    def w3(p, kind, side):
        ref = (up, down)[kind]
        rows = piece(z, p)
        dev = at(x, y, m4(z + (1, -1)[side]), core)
        return remote(ref.at[rows], ref.at[rows], w3s.at[side, kind, p], w3r.at[side, kind, p], dev)

    def w3_got(p, kind, side):
        ref = (up, down)[kind]
        rows = piece(m4(z - (1, -1)[side]), p)
        dev = at(x, y, m4(z - (1, -1)[side]), core)
        return remote(ref.at[rows], ref.at[rows], w3s.at[side, kind, p], w3r.at[side, kind, p], dev)

    def w3f(p, side):
        ref = (up, down)[side]
        rows = piece(m4(z - (1, -1)[side]), p)
        dev = at(x, y, m4(z + (1, -1)[side]), core)
        return remote(ref.at[rows], ref.at[rows], w3fs.at[side, p], w3fr.at[side, p], dev)

    def w3f_got(p, side):
        ref = (up, down)[side]
        rows = piece(m4(z + 2), p)
        dev = at(x, y, m4(z - (1, -1)[side]), core)
        return remote(ref.at[rows], ref.at[rows], w3fs.at[side, p], w3fr.at[side, p], dev)

    def w4(zz, p, kind):
        ref = (up, down)[kind]
        rows = piece(zz, p)
        dev = at(x, y, z, 1 - core)
        return remote(ref.at[rows], ref.at[rows], w4s.at[kind, zz, p], w4r.at[kind, zz, p], dev)

    def w4_got(zz, p, kind):
        ref = (up, down)[kind]
        rows = pl.ds(pl.multiple_of(((zz * 4 + p) * 2 + 1 - core) * 64, 64), 64)
        dev = at(x, y, z, 1 - core)
        return remote(ref.at[rows], ref.at[rows], w4s.at[kind, zz, p], w4r.at[kind, zz, p], dev)

    for d in range(1, 8):
        j = lax.rem(me + d, 8)
        remote(s3.at[j], m_in.at[part(j)], s3s.at[j], s3r.at[j], (z * 8 + j, x)).wait_recv()

    def own_pieces(d):
        p = m4(y + d)
        if d:
            for kind in (0, 1):
                ref = (up, down)[kind]
                rows = piece(z, p)
                remote(
                    ref.at[rows], ref.at[rows], w2s.at[kind, p], w2r.at[kind, p], at(x, p, z, core)
                ).wait_recv()
        for kind, side in ((0, 0), (1, 1), (1, 0), (0, 1)):
            w3(p, kind, side).start()
        for kind in (0, 1):
            w4(z, p, kind).start()

    def near_pieces(p):
        for kind in (0, 1):
            w3_got(p, kind, kind).wait_recv()
            w3f(p, kind).start()
        for kind in (0, 1):
            w3_got(p, kind, 1 - kind).wait_recv()
        for kind in (0, 1):
            w4(m4(z + 1), p, kind).start()
            w4(m4(z - 1), p, kind).start()

    def far_pieces(p):
        for kind in (0, 1):
            w3f_got(p, kind).wait_recv()
        for kind in (0, 1):
            w4(m4(z + 2), p, kind).start()

    for c in loads[10:]:
        c.wait()

    low, high = slice(0, H), slice(H, D)

    class Ring:
        def __init__(self, coord, dev, p, ra, rb, a_s, a_r, b_s, b_r):
            self.c, self.dev, self.p, self.ra, self.rb = coord, dev, p, ra, rb
            self.a_s, self.a_r, self.b_s, self.b_r = a_s, a_r, b_s, b_r

        def up_of(self, k):
            return m4(self.c + k)

        def relay(self, s, side):
            far = self.p.at[s, self.up_of(2), :, (high, low)[side]]
            dev = self.dev(self.up_of((1, -1)[side]))
            return remote(far, self.ra.at[s, side], self.a_s.at[s, side], self.a_r.at[s, side], dev)

        def near(self, s, side, half):
            t = self.up_of((1, -1)[side])
            cols = (low, high)[half]
            return remote(
                self.p.at[s, t, :, cols], self.rb.at[s, side, :, cols],
                self.b_s.at[s, side, half], self.b_r.at[s, side, half], self.dev(t),
            )

        def begin(self, s):
            for side in (0, 1):
                self.relay(s, side).start()
            for side in (0, 1):
                self.near(s, side, side).start()

        def middle(self, s):
            for side in (0, 1):
                self.relay(s, side).wait_recv()
                t = self.up_of((1, -1)[side])
                cols = (high, low)[side]
                self.p[s, t, :, cols] = (
                    self.p[s, t, :, cols].astype(F32) + self.ra[s, side].astype(F32)
                ).astype(BF16)
                self.near(s, side, 1 - side).start()

        def end(self, s):
            for side in (0, 1):
                for half in (0, 1):
                    self.near(s, side, half).wait_recv()
            return (
                self.p[s, self.c].astype(F32)
                + self.rb[s, 0].astype(F32)
                + self.rb[s, 1].astype(F32)
            )

        def drain(self, s):
            for side in (0, 1):
                self.relay(s, side).wait_send()
                for half in (0, 1):
                    self.near(s, side, half).wait_send()

    ring_x = Ring(x, lambda t: at(t, y, z, core), px, rxa, rxb, xas, xar, xbs, xbr)
    ring_y = Ring(y, lambda t: at(x, t, z, core), py, rya, ryb, yas, yar, ybs, ybr)

    def ag(s, side, half):
        cols = (low, high)[half]
        dev = at(x, m4(y + (1, -1)[side]), z, core)
        return remote(
            xs.at[s, y, :, cols], xs.at[s, y, :, cols],
            ags.at[s, side, half], agr.at[s, side, half], dev,
        )

    def ag_got(s, side, half):
        cols = (low, high)[half]
        b = m4(y - (1, -1)[side])
        return remote(
            xs.at[s, b, :, cols], xs.at[s, b, :, cols],
            ags.at[s, side, half], agr.at[s, side, half], at(x, b, z, core),
        )

    def af(s, side):
        cols = (low, high)[side]
        b = m4(y - (1, -1)[side])
        dev = at(x, m4(y + (1, -1)[side]), z, core)
        return remote(
            xs.at[s, b, :, cols], xs.at[s, b, :, cols], afs.at[s, side], afr.at[s, side], dev
        )

    def af_got(s, side):
        cols = (low, high)[side]
        b = m4(y + 2)
        return remote(
            xs.at[s, b, :, cols], xs.at[s, b, :, cols], afs.at[s, side], afr.at[s, side],
            at(x, m4(y - (1, -1)[side]), z, core),
        )

    def oa(s, d):
        t = m4(x + d)
        cols = pl.ds(pl.multiple_of(t * 512, 512), 512)
        return remote(
            fin.at[s, :, cols], outb.at[x, s], oas.at[s, t], oar.at[s, x], at(t, y, z, core)
        )

    def oa_got(s, d):
        t = m4(x + d)
        cols = pl.ds(pl.multiple_of(x * 512, 512), 512)
        return remote(
            fin.at[s, :, cols], outb.at[t, s], oas.at[s, t], oar.at[s, t], at(t, y, z, core)
        )

    def od(s, t):
        return pltpu.make_async_copy(
            outb.at[t, s], out.at[pl.ds(pl.multiple_of((t * S + s) * R, R), R)], ods.at[t, s]
        )

    def project(s):
        blocks = []
        for t in range(4):
            rows = pl.ds(pl.multiple_of((t * S + s) * R, R), R)
            sides = []
            for ks, vs in ((slice(0, KA), slice(0, 512)), (slice(KA, KK), slice(512, 1024))):
                a = att[rows, vs] + dot_nt(qo[rows, ks], m_in[:, ks])
                norm = lax.rsqrt(jnp.mean(jnp.square(a), axis=1, keepdims=True) + EPS)
                u = g_s[rows, vs].astype(F32)
                a = a * norm * gain[...] * (u / (1.0 + jnp.exp(-u)))
                sides.append(a.astype(BF16))
            blocks.append(jnp.concatenate(sides, axis=1))
        gated = jnp.concatenate(blocks, axis=0)
        for n in range(4):
            cols = slice(512 * n, 512 * n + 512)
            r = dot(gated, o_s[:, cols]).astype(BF16)
            px[s, :, :, cols] = r.reshape(4, R, 512)

    def normalize(s):
        mixed = ring_x.end(s)
        rows = pl.ds(pl.multiple_of(s * R, R), R)
        stream = (res_s[rows, :].astype(F32) + mixed).astype(BF16)
        st[s] = stream
        f = stream.astype(F32)
        norm = lax.rsqrt(jnp.mean(jnp.square(f), axis=1, keepdims=True) + EPS)
        xs[s, y] = (f * norm * mgain[...]).astype(BF16)
        for half in (0, 1):
            for side in (0, 1):
                ag(s, side, half if side == 0 else 1 - half).start()

    def mix(s):
        rows = xs[s].reshape(4 * R, D)
        for n in range(2):
            cols = slice(512 * n, 512 * n + 512)
            h = jnp.maximum(dot(rows, up[:, cols]), 0.0)
            hid[:, cols] = (h * h).astype(BF16)
        for n in range(4):
            cols = slice(512 * n, 512 * n + 512)
            r = dot_nt(hid[...], down[cols, :]).astype(BF16)
            py[s, :, :, cols] = r.reshape(4, R, 512)

    def tick(tau, _):
        def stage(k, f):
            @pl.when((tau >= k) & (tau < k + S))
            def _():
                f(tau - k)

        def a_stage(s):
            project(s)
            ring_x.begin(s)

        def d_stage(s):
            for side in (0, 1):
                ag_got(s, side, side).wait_recv()
                af(s, side).start()

        def e_stage(s):
            @pl.when(s == 0)
            def _():
                for zz in range(4):
                    for p in range(4):
                        for kind in (0, 1):
                            w4_got(zz, p, kind).wait_recv()

            for side in (0, 1):
                ag_got(s, side, 1 - side).wait_recv()
                af_got(s, side).wait_recv()
            mix(s)
            ring_y.begin(s)

        def g_stage(s):
            fin[s] = (ring_y.end(s) + st[s].astype(F32)).astype(BF16)
            for d in (1, 3, 2):
                oa(s, d).start()
            outb[x, s] = fin[s, :, pl.ds(pl.multiple_of(x * 512, 512), 512)]
            od(s, x).start()

        def h_stage(s):
            for d in (1, 2, 3):
                oa_got(s, d).wait_recv()
                od(s, m4(x + d)).start()

        stage(0, a_stage)
        stage(0, near_pieces)
        stage(1, ring_x.middle)
        stage(1, far_pieces)
        stage(2, normalize)
        stage(3, d_stage)
        stage(4, e_stage)
        stage(5, ring_y.middle)
        stage(6, g_stage)
        stage(7, h_stage)
        return 0

    for d in range(4):
        own_pieces(d)
    lax.fori_loop(0, S + 7, tick, 0)

    for d in (1, 2, 3):
        w1(d).wait_send()
        for c in w2(d) + s2(d):
            c.wait_send()
    for d in range(1, 8):
        for c in s1(d) + (s3c(d),):
            c.wait_send()

    def drain(s, _):
        for kind in (0, 1):
            for side in (0, 1):
                w3(s, kind, side).wait_send()
            w3f(s, kind).wait_send()
            for zz in range(4):
                w4(zz, s, kind).wait_send()
        ring_x.drain(s)
        ring_y.drain(s)
        for side in (0, 1):
            for half in (0, 1):
                ag(s, side, half).wait_send()
            af(s, side).wait_send()
        for d in (1, 2, 3):
            oa(s, d).wait_send()
        for t in range(4):
            od(s, t).wait()
        return 0

    lax.fori_loop(0, S, drain, 0)


def body(
    residual, query_wide, key_wide, value_wide, decay_wide, gate_wide, query_narrow, key_narrow,
    value_narrow, decay_narrow, gate_narrow, head_gain, out_wide, out_narrow, mlp_gain,
    up_weight, down_weight,
):
    def v(*shape, dtype=BF16):
        return pltpu.VMEM(shape, dtype)

    def sem(*shape):
        return pltpu.SemaphoreType.DMA(shape)

    any_space = pl.BlockSpec(memory_space=pl.ANY)
    vmem = pl.BlockSpec(memory_space=pltpu.VMEM)
    scratch = [
        v(1024, KK), v(1024, KK), v(1024, KK), v(1024, 1024), v(1024, 1024), v(1024, D), v(S * R, D),
        v(4, 128, H), v(D, H), v(D, H), v(1024, KK), v(1024, KK), v(CH, 512, KK),
        v(512, KK, dtype=F32), v(512, KK), v(8, KK, dtype=F32),
        v(8, 64, KK), v(8, 8, KK, dtype=F32), v(64, KK), v(8, KK, dtype=F32),
        v(4, 64, KK), v(4, 8, KK, dtype=F32), v(8, 64, KK), v(512, KK), v(1024, 1024, dtype=F32),
        v(S, 4, R, D), v(S, 2, R, H), v(S, 2, R, D), v(S, R, D), v(S, 4, R, D),
        v(S, 4, R, D), v(S, 2, R, H), v(S, 2, R, D), v(4 * R, H), v(S, R, D), v(4, S, R, 512),
        sem(15), sem(4), sem(4), sem(2, 4), sem(2, 4), sem(2, 2, 4), sem(2, 2, 4),
        sem(2, 4), sem(2, 4), sem(2, 4, 4), sem(2, 4, 4),
        sem(8), sem(8), sem(8), sem(8), sem(4), sem(4), sem(4), sem(4), sem(8), sem(8),
        sem(S, 2), sem(S, 2), sem(S, 2, 2), sem(S, 2, 2),
        sem(S, 2), sem(S, 2), sem(S, 2, 2), sem(S, 2, 2),
        sem(S, 2, 2), sem(S, 2, 2), sem(S, 2), sem(S, 2), sem(S, 4), sem(S, 4), sem(4, S),
    ]
    return pl.pallas_call(
        kernel,
        out_shape=jax.ShapeDtypeStruct((1024, 512), BF16),
        in_specs=[any_space] * 15 + [vmem] * 2,
        out_specs=any_space,
        scratch_shapes=scratch,
        compiler_params=pltpu.CompilerParams(
            collective_id=0, has_side_effects=True, vmem_limit_bytes=67_000_000
        ),
    )(
        residual, query_wide, key_wide, value_wide, decay_wide, gate_wide, query_narrow, key_narrow,
        value_narrow, decay_narrow, gate_narrow, out_wide, out_narrow, up_weight, down_weight.T,
        head_gain.reshape(1, -1), mlp_gain.reshape(1, -1),
    )


def solution(mesh):
    return jax.shard_map(
        body,
        mesh=mesh,
        in_specs=(
            P("sp", None),
            *[P("sp", "tp")] * 10,
            P(),
            P("tp", None),
            P("tp", None),
            P(),
            P("sp", "tp"),
            P("tp", "sp"),
        ),
        out_specs=P("sp", "tp"),
        check_vma=False,
    )
```

time: 545 us -> 152 us (0.28)
  waiting for transfers between devices: 164 us -> 0 us
  Pallas kernels: 0 us -> 149 us
  blocking collectives: 98.6 us -> 0 us
  matrix products: 91.9 us -> 0 us
  local copies, waits for them, and re-layouts: 86.4 us -> 2.26 us
  other arithmetic: 74.3 us -> 0 us
  between operations: 13.5 us -> 0.01 us
  starting transfers between devices: 8.53 us -> 0 us
    pallas_call x0 -> x1, Pallas kernels: none -> 149 us  [body(): pl.pallas_call(kernel, out_shape=jax.ShapeDtypeStruct((1024, 512), BF16),...]
    all_gather x4 -> x0, waiting for transfers between devices: 111 us -> none  [the longest x1 111 us: body(): normed = lax.all_gather(normed_cols, 'tp', axis=1, tiled=True)]
    dot_general x134 -> x0, matrix products: 91.9 us -> none  [the longest x32 22.1 us: advance(): outside = jnp.einsum('ihd,hde->ihe', scaled_q, memory, precision=HIGHEST)]
    all_to_all x2 -> x0, waiting for transfers between devices: 53 us -> none  [the longest x1 48.5 us: sum_at_owner(): pieces = lax.all_to_all(split_up(array, dim, count), axis, 0, 0, tiled=True)]
    all_to_all x1 -> x0, blocking collectives: 51.8 us -> none  [sum_at_owner(): pieces = lax.all_to_all(split_up(array, dim, count), axis, 0, 0, tiled=True)]
    all_gather x2 -> x0, blocking collectives: 46.9 us -> none  [entering(): lax.all_gather(a.astype(kind), axis)]
    dynamic_slice x49 -> x0, local copies, waits for them, and re-layouts: 42.4 us -> none  [the longest x48 41.7 us: block_pass(): lax.scan(advance, initial, (to_blocks(queries), to_blocks(keys_in), to_bl...]
    mul x34 -> x0, other arithmetic: 33.1 us -> none  [the longest x16 17 us: advance(): carried_q = scaled_q * jnp.exp(offset)[None]]
  transfers between devices with their start and end apart: 6 -> 0, of which waited for: 3 -> 0; matrix products, arithmetic and copies ran while one was open for 30% -> 0% of each run, Pallas kernels for 0% -> 0%
where the time goes in v1:
time: 152 us; the launch traced here: 151 us
  Pallas kernels  149 us (98%)
  local copies, waits for them, and re-layouts  2.26 us (1%)
    pallas_call x1, Pallas kernels, body(): pl.pallas_call(kernel, out_shape=jax.ShapeDtypeStruct((1024, 512), BF16),...  149 us

profile of v1, /device:TPU:0, one launch (start us, length us, event | category | flops | bytes accessed | tf_op | source)
XLA Modules:
  0.0 151.4 jit_solution(11816614113477249445)
XLA Ops:
  0.0 149.1 %shard_map.163 = bf16[1024,512]{1,0:T(8,128)(2,1)} custom-call(bf16[1024,2048]{1,0:T(8,128)(2,1)} %res.1, bf16[1024,256]{1,0:T(8,128)(2,1)} %qw.1, bf16[1024,256]{1,0:T(8,128)(2,1)} %kw.1, bf16[1024,512]{1,0:T(8,128)(2,1)} %vw.1, bf16[1024,256]{1,0:T(8,128)(2,1)} %dw.1, bf16[1024,512]{1,0:T(8,128)(2,1)} %gw.1, bf16[1024,128]{1,0:T(8,128)(2,1)} %qn.1, ...), custom_call_target="tpu_custom_call" | custom-call | tf_op jit(solution)/shard_map/pallas_call | solution.py:577
  149.1 2.3 %copy.19 = bf16[1024,512]{1,0:T(8,128)(2,1)} copy(bf16[1024,512]{1,0:T(8,128)(2,1)} %shard_map.163) | data formatting | bytes 2097152

commit v2 on v1

v2 whole, which is shorter than its diff:
```python
import jax
import jax.numpy as jnp
from jax import lax
from jax.experimental import pallas as pl
from jax.experimental.pallas import tpu as pltpu
from jax.sharding import PartitionSpec as P

MESH = pl.DeviceIdType.MESH
F32, BF16 = jnp.float32, jnp.bfloat16
EPS = 1e-05
C = 128
CH = 8
KA, KB, KK = 256, 128, 384
S = 8
R = 256 // S
SX = S - S // 4
BO, CO, DO, EO, FO, GO, HO = 2, 4, 5, 9, 11, 13, 15
W_TICKS = ((0, None, 1, 4), (1, None, 3, 5), (3, None, 4, 6), (2, 5, 7, 8))
D = 2048
H = 1024


def dot(a, b):
    return jnp.dot(a, b, preferred_element_type=F32)


def dot_nt(a, b):
    return lax.dot_general(a, b, (((1,), (1,)), ((), ())), preferred_element_type=F32)


def dot_tn(a, b):
    return lax.dot_general(a, b, (((0,), (0,)), ((), ())), preferred_element_type=F32)


def kernel(
    res, qw, kw, vw, dw, gw, qn, kn, vn, dn, gn, ow, on, upw, dnw, gain, mgain,
    out,
    q_s, k_s, d_s, v_s, g_s, o_s, res_s, xw, xw2, up, down, wi, offs, qo, mc, m_s, sb, dt,
    r1, rd1, t2, dt2, r2, rd2, s3, m_in, att, px, rxa, rxb, st, xs, py, rya, ryb, hid, fin, outb,
    ld, w1s, w1r, w2s, w2r, w3s, w3r, w3fr, w4s, w4r, ss, sr,
    xs_s, xar, xbr, ys_s, yar, ybr, ags, agr, afr, oas, oar, ods,
):
    sp = lax.axis_index("sp")
    x = lax.axis_index("tp")
    core = lax.rem(sp, 2)
    y = lax.rem(lax.div(sp, 2), 4)
    z = lax.div(sp, 8)
    me = lax.rem(sp, 8)

    def at(xx, yy, zz, cc):
        return ((zz * 4 + yy) * 2 + cc, xx)

    def m4(v):
        return lax.rem(v + 8, 4)

    def remote(src, dst, ss, rs, dev):
        return pltpu.make_async_remote_copy(
            src_ref=src, dst_ref=dst, send_sem=ss, recv_sem=rs, device_id=dev, device_id_type=MESH
        )

    def got(ref, sem):
        pltpu.make_async_copy(ref, ref, sem).wait()

    tok = pl.ds(pl.multiple_of(x * (S * R), S * R), S * R)
    loads = [
        (upw, xw.at[0:64]),
        (dnw, xw.at[64:128]),
        (dw, d_s.at[:, 0:KA]),
        (dn, d_s.at[:, KA:KK]),
        (kw, k_s.at[:, 0:KA]),
        (kn, k_s.at[:, KA:KK]),
        (vw, v_s.at[:, 0:512]),
        (vn, v_s.at[:, 512:1024]),
        (qw, q_s.at[:, 0:KA]),
        (qn, q_s.at[:, KA:KK]),
        (gw, g_s.at[:, 0:512]),
        (gn, g_s.at[:, 512:1024]),
        (ow, o_s.at[0:512]),
        (on, o_s.at[512:1024]),
        (res.at[tok], res_s),
    ]
    groups = (0, 0, 1, 1, 2, 2, 3, 3, 4, 4, 5, 5, 6, 6, 7)
    for (a, b), i in zip(loads, groups):
        pltpu.make_async_copy(a, b, ld.at[i]).start()

    barrier = pltpu.get_barrier_semaphore()
    for d in (1, 2, 3):
        pl.semaphore_signal(barrier, inc=1, device_id=at(m4(x + d), y, z, core), device_id_type=MESH)
        pl.semaphore_signal(barrier, inc=1, device_id=at(x, y, m4(z + d), core), device_id_type=MESH)
    for d in range(1, 8):
        j = lax.rem(me + d, 8)
        pl.semaphore_signal(barrier, inc=1, device_id=(z * 8 + j, x), device_id_type=MESH)
    for d in (1, 3):
        for dev in (at(m4(x - y - d), m4(y + d), z, core), at(m4(x + y), m4(y + d), z, core)):
            pl.semaphore_signal(barrier, inc=1, device_id=dev, device_id_type=MESH)

    own = pl.ds(pl.multiple_of(sp * 64, 64), 64)

    def w2(d):
        src = xw2 if d == 2 else xw
        dev = at(x if d == 2 else m4(x - y - d), m4(y + d), z, core)
        return (
            remote(src.at[0:64], up.at[own], w2s.at[min(d, 1)], w2r.at[y], dev),
            remote(src.at[64:128], down.at[own], w2s.at[min(d, 1)], w2r.at[y], dev),
        )

    w1 = remote(xw, xw2, w1s.at[0], w1r.at[0], at(m4(x - y - 2), y, z, core))

    def w2_start(d):
        for c in w2(d):
            if d:
                c.start()
            else:
                pl.when(y != 0)(c.start)

    row_i = lax.broadcasted_iota(jnp.int32, (C, C), 0)
    col_i = lax.broadcasted_iota(jnp.int32, (C, C), 1)
    causal = col_i <= row_i
    lower = causal.astype(BF16)
    lane = lax.broadcasted_iota(jnp.int32, (1, KK), 1)
    scale = jnp.where(lane < KA, KA**-0.5, KB**-0.5).astype(F32)
    got(d_s, ld.at[1])
    got(k_s, ld.at[2])
    got(v_s, ld.at[3])
    m_s[...] = jnp.zeros_like(m_s)

    def first(c, off):
        rows = pl.ds(pl.multiple_of(c * C, C), C)
        dd = d_s[rows, :].astype(F32)
        g = (jnp.minimum(dd, 0.0) - jnp.log1p(jnp.exp(-jnp.abs(dd)))) * (1.0 / 16.0)
        high = g.astype(BF16)
        low = (g - high.astype(F32)).astype(BF16)
        within = dot(lower, high) + dot(lower, low)
        last = within[C - 1 : C, :]
        wi[rows, :] = within
        offs[c] = off
        kd = (k_s[rows, :].astype(F32) * jnp.exp(last - within)).astype(BF16)
        mc[c] = m_s[...].astype(BF16)
        fade = jnp.exp(last)
        m_s[:, 0:KA] = m_s[:, 0:KA] * fade[:, 0:KA] + dot_tn(v_s[rows, 0:512], kd[:, 0:KA])
        m_s[:, KA:KK] = m_s[:, KA:KK] * fade[:, KA:KK] + dot_tn(v_s[rows, 512:1024], kd[:, KA:KK])
        return off + last

    total = lax.fori_loop(0, CH // 2, first, jnp.zeros((1, KK), F32))
    pl.semaphore_wait(barrier, 17)
    got(xw, ld.at[0])
    w2_start(0)
    pl.when(y != 2)(w1.start)

    @pl.when(y == 2)
    def _():
        xw2[...] = xw[...]

    total = lax.fori_loop(CH // 2, CH, first, total)
    sb[...] = m_s[...].astype(BF16)
    dt[...] = total

    def part(j):
        return pl.ds(pl.multiple_of(j * 64, 64), 64)

    def s1(d):
        j = lax.rem(me + d, 8)
        dev = (z * 8 + j, x)
        return (
            remote(sb.at[part(j)], r1.at[me], ss.at[0], sr.at[0], dev),
            remote(dt, rd1.at[me], ss.at[1], sr.at[1], dev),
        )

    for d in range(1, 8):
        for c in s1(d):
            c.start()
    r1[me] = sb[part(me), :]
    rd1[me] = dt[...]

    def piece(zz, p):
        return pl.ds(pl.multiple_of(((zz * 4 + p) * 2 + core) * 64, 64), 64)

    def w3(p, kind, side):
        ref = (up, down)[kind]
        rows = piece(z, p)
        dev = at(x, y, m4(z + (1, -1)[side]), core)
        return remote(ref.at[rows], ref.at[rows], w3s.at[0], w3r.at[p], dev)

    def w3f(p, side):
        ref = (up, down)[side]
        rows = piece(m4(z - (1, -1)[side]), p)
        dev = at(x, y, m4(z + (1, -1)[side]), core)
        return remote(ref.at[rows], ref.at[rows], w3s.at[0], w3fr.at[p], dev)

    def w4(zz, p, kind):
        ref = (up, down)[kind]
        rows = piece(zz, p)
        dev = at(x, y, z, 1 - core)
        return remote(ref.at[rows], ref.at[rows], w4s.at[0], w4r.at[0], dev)

    def own_piece(d):
        p = m4(y + d)
        if d:
            got(up.at[0:128], w2r.at[p])
        else:

            @pl.when(y != 0)
            def _():
                got(up.at[0:128], w2r.at[p])

            @pl.when(y == 0)
            def _():
                up[own, :] = xw[0:64]
                down[own, :] = xw[64:128]

        for kind, side in ((0, 0), (1, 1), (1, 0), (0, 1)):
            w3(p, kind, side).start()
        for kind in (0, 1):
            w4(z, p, kind).start()

    def near_pieces(d):
        p = m4(y + d)
        got(up.at[0:256], w3r.at[p])
        for kind in (0, 1):
            w3f(p, kind).start()
        for kind in (0, 1):
            w4(m4(z + 1), p, kind).start()
            w4(m4(z - 1), p, kind).start()

    def far_pieces(d):
        p = m4(y + d)
        got(up.at[0:128], w3fr.at[p])
        for kind in (0, 1):
            w4(m4(z + 2), p, kind).start()

    def second(c, _):
        rows = pl.ds(pl.multiple_of(c * C, C), C)
        within = wi[rows, :]
        rel = within - within[C // 2 - 1 : C // 2, :]
        qf = q_s[rows, :].astype(F32) * scale
        decayed = qf * jnp.exp(within)
        qt = (qf * jnp.exp(rel)).astype(BF16)
        kt = (k_s[rows, :].astype(F32) * jnp.exp(-rel)).astype(BF16)
        qdec = decayed.astype(BF16)
        qo[rows, :] = (decayed * jnp.exp(offs[c])).astype(BF16)
        for ks, vs in ((slice(0, KA), slice(0, 512)), (slice(KA, KK), slice(512, 1024))):
            sc = dot_nt(qt[:, ks], kt[:, ks])
            sc = jnp.where(causal, sc, 0.0).astype(BF16)
            att[rows, vs] = dot(sc, v_s[rows, vs]) + dot_nt(qdec[:, ks], mc[c, :, ks])
        return 0

    got(q_s, ld.at[4])
    lax.fori_loop(0, CH, second, 0)

    got(r1.at[0:7], sr.at[0])
    got(rd1.at[0:7], sr.at[1])

    def over_cores(j, carry):
        acc, dacc = carry
        dj = rd1[j]
        return acc * jnp.exp(dj) + r1[j].astype(F32), dacc + dj

    acc, dacc = lax.fori_loop(
        0, 8, over_cores, (jnp.zeros((64, KK), F32), jnp.zeros((1, KK), F32))
    )
    t2[...] = acc.astype(BF16)
    dt2[...] = dacc

    def s2(d):
        t = m4(z + d)
        dev = at(x, y, t, core)
        return (
            remote(t2, r2.at[z], ss.at[2], sr.at[2], dev),
            remote(dt2, rd2.at[z], ss.at[3], sr.at[3], dev),
        )

    for d in (1, 3, 2):
        for c in s2(d):
            c.start()
    r2[z] = t2[...]
    rd2[z] = dt2[...]
    w2_start(1)
    w2_start(3)
    own_piece(0)
    got(r2.at[0:3], sr.at[2])
    got(rd2.at[0:3], sr.at[3])

    def over_z(t, acc):
        return jnp.where(t < z, acc * jnp.exp(rd2[t]) + r2[t].astype(F32), acc)

    acc = lax.fori_loop(0, 4, over_z, jnp.zeros((64, KK), F32))

    def hand_out(j, acc):
        s3[j] = acc.astype(BF16)
        return acc * jnp.exp(rd1[j]) + r1[j].astype(F32)

    lax.fori_loop(0, 8, hand_out, acc)

    def s3c(d):
        j = lax.rem(me + d, 8)
        return remote(s3.at[j], m_in.at[part(me)], ss.at[4], sr.at[4], (z * 8 + j, x))

    for d in range(1, 8):
        s3c(d).start()
    m_in[part(me), :] = s3[me]
    own_piece(1)
    own_piece(3)

    got(m_in.at[0:448], sr.at[4])

    pl.when(y != 2)(w1.wait_recv)
    w2_start(2)
    got(g_s, ld.at[5])
    got(o_s, ld.at[6])
    got(res_s, ld.at[7])

    low, high = slice(0, H), slice(H, D)

    class Ring:
        def __init__(self, coord, dev, p, ra, rb, sends, a_r, b_r):
            self.c, self.dev, self.p, self.ra, self.rb = coord, dev, p, ra, rb
            self.sends, self.a_r, self.b_r = sends, a_r, b_r

        def up_of(self, s, k):
            return m4(self.c(s) + k)

        def relay(self, s, side):
            far = self.p.at[s, self.up_of(s, 2), :, (high, low)[side]]
            dev = self.dev(s, self.up_of(s, (1, -1)[side]))
            return remote(far, self.ra.at[s, side], self.sends.at[0], self.a_r.at[s], dev)

        def near(self, s, side, half):
            t = self.up_of(s, (1, -1)[side])
            cols = (low, high)[half]
            return remote(
                self.p.at[s, t, :, cols], self.rb.at[s, side, :, cols],
                self.sends.at[0], self.b_r.at[s], self.dev(s, t),
            )

        def begin(self, s):
            for side in (0, 1):
                self.relay(s, side).start()
            for side in (0, 1):
                self.near(s, side, side).start()

        def middle(self, s):
            got(self.ra.at[s], self.a_r.at[s])
            for side in (0, 1):
                t = self.up_of(s, (1, -1)[side])
                cols = (high, low)[side]
                self.p[s, t, :, cols] = (
                    self.p[s, t, :, cols].astype(F32) + self.ra[s, side].astype(F32)
                ).astype(BF16)
                self.near(s, side, 1 - side).start()

        def end(self, s):
            got(self.rb.at[s], self.b_r.at[s])
            return (
                self.p[s, self.c(s)].astype(F32)
                + self.rb[s, 0].astype(F32)
                + self.rb[s, 1].astype(F32)
            )

    def place(s):
        return jnp.where(s >= SX, x, y)

    def member(s, t):
        return at(jnp.where(s >= SX, t, x), jnp.where(s >= SX, y, t), z, core)

    ring_x = Ring(lambda s: x, lambda s, t: at(t, y, z, core), px, rxa, rxb, xs_s, xar, xbr)
    ring_y = Ring(place, member, py, rya, ryb, ys_s, yar, ybr)

    def ag(s, side, half):
        cols = (low, high)[half]
        a = place(s)
        return remote(
            xs.at[s, a, :, cols], xs.at[s, a, :, cols],
            ags.at[0], (agr if side == half else afr).at[s], member(s, m4(a + (1, -1)[side])),
        )

    def af(s, side):
        cols = (low, high)[side]
        b = m4(place(s) - (1, -1)[side])
        return remote(
            xs.at[s, b, :, cols], xs.at[s, b, :, cols],
            ags.at[0], afr.at[s], member(s, m4(place(s) + (1, -1)[side])),
        )

    def oa(s, d):
        t = m4(x + d)
        cols = pl.ds(pl.multiple_of(t * 512, 512), 512)
        return remote(
            fin.at[s, :, cols], outb.at[x, s], oas.at[0], oar.at[s], at(t, y, z, core)
        )

    def od(s, t):
        return pltpu.make_async_copy(
            outb.at[t, s], out.at[pl.ds(pl.multiple_of((t * S + s) * R, R), R)], ods.at[0]
        )

    def project(s):
        blocks = []
        for t in range(4):
            rows = pl.ds(pl.multiple_of((t * S + s) * R, R), R)
            sides = []
            for ks, vs in ((slice(0, KA), slice(0, 512)), (slice(KA, KK), slice(512, 1024))):
                a = att[rows, vs] + dot_nt(qo[rows, ks], m_in[:, ks])
                norm = lax.rsqrt(jnp.mean(jnp.square(a), axis=1, keepdims=True) + EPS)
                u = g_s[rows, vs].astype(F32)
                a = a * norm * gain[...] * (u / (1.0 + jnp.exp(-u)))
                sides.append(a.astype(BF16))
            blocks.append(jnp.concatenate(sides, axis=1))
        gated = jnp.concatenate(blocks, axis=0)
        for n in range(4):
            cols = slice(512 * n, 512 * n + 512)
            r = dot(gated, o_s[:, cols]).astype(BF16)
            px[s, :, :, cols] = r.reshape(4, R, 512)

    def normalize(s):
        mixed = ring_x.end(s)
        rows = pl.ds(pl.multiple_of(s * R, R), R)
        stream = (res_s[rows, :].astype(F32) + mixed).astype(BF16)
        st[s] = stream
        f = stream.astype(F32)
        norm = lax.rsqrt(jnp.mean(jnp.square(f), axis=1, keepdims=True) + EPS)
        xs[s, place(s)] = (f * norm * mgain[...]).astype(BF16)
        for half in (0, 1):
            for side in (0, 1):
                ag(s, side, half if side == 0 else 1 - half).start()

    def mix(s):
        rows = xs[s].reshape(4 * R, D)
        for n in range(2):
            cols = slice(512 * n, 512 * n + 512)
            h = jnp.maximum(dot(rows, up[:, cols]), 0.0)
            hid[:, cols] = (h * h).astype(BF16)
        for n in range(4):
            cols = slice(512 * n, 512 * n + 512)
            r = dot_nt(hid[...], down[cols, :]).astype(BF16)
            py[s, :, :, cols] = r.reshape(4, R, 512)

    def tick(tau, _):
        def stage(k, f):
            @pl.when((tau >= k) & (tau < k + S))
            def _():
                f(tau - k)

        def once(k, f, d):
            @pl.when(tau == k)
            def _():
                f(d)

        def a_stage(s):
            project(s)
            ring_x.begin(s)

        def d_stage(s):
            got(rya.at[s], agr.at[s])
            for side in (0, 1):
                af(s, side).start()

        def e_stage(s):
            @pl.when(s == 0)
            def _():
                got(up, w4r.at[0])

            got(ryb.at[s], afr.at[s])
            mix(s)
            ring_y.begin(s)

        def g_stage(s):
            fin[s] = (ring_y.end(s) + st[s].astype(F32)).astype(BF16)
            for d in (1, 3, 2):
                oa(s, d).start()
            outb[x, s] = fin[s, :, pl.ds(pl.multiple_of(x * 512, 512), 512)]
            od(s, x).start()

        def h_stage(s):
            got(outb.at[0:3, s], oar.at[s])
            for d in (1, 2, 3):
                od(s, m4(x + d)).start()

        stage(0, a_stage)
        for d, mine, near, far in W_TICKS:
            if mine is not None:
                once(mine, own_piece, d)
        for d, mine, near, far in W_TICKS:
            once(near, near_pieces, d)
        for d, mine, near, far in W_TICKS:
            once(far, far_pieces, d)
        stage(BO, ring_x.middle)
        stage(CO, normalize)
        stage(DO, d_stage)
        stage(EO, e_stage)
        stage(FO, ring_y.middle)
        stage(GO, g_stage)
        stage(HO, h_stage)
        return 0

    lax.fori_loop(0, S + HO, tick, 0)

    @pl.when(y != 0)
    def _():
        got(up.at[0:128], w2s.at[0])

    pl.when(y != 2)(w1.wait_send)
    got(up.at[0:384], w2s.at[1])
    got(r1.at[0:7], ss.at[0])
    got(rd1.at[0:7], ss.at[1])
    got(r2.at[0:3], ss.at[2])
    got(rd2.at[0:3], ss.at[3])
    got(m_in.at[0:448], ss.at[4])
    got(up.at[0:1536], w3s.at[0])
    got(up, w4s.at[0])
    for sends in (xs_s, ys_s, ags):
        got(up.at[0:1536], sends.at[0])
    got(outb.at[0:3], oas.at[0])
    got(outb, ods.at[0])


def body(
    residual, query_wide, key_wide, value_wide, decay_wide, gate_wide, query_narrow, key_narrow,
    value_narrow, decay_narrow, gate_narrow, head_gain, out_wide, out_narrow, mlp_gain,
    up_weight, down_weight,
):
    def v(*shape, dtype=BF16):
        return pltpu.VMEM(shape, dtype)

    def sem(*shape):
        return pltpu.SemaphoreType.DMA(shape)

    any_space = pl.BlockSpec(memory_space=pl.ANY)
    vmem = pl.BlockSpec(memory_space=pltpu.VMEM)
    scratch = [
        v(1024, KK), v(1024, KK), v(1024, KK), v(1024, 1024), v(1024, 1024), v(1024, D), v(S * R, D),
        v(128, H), v(128, H), v(D, H), v(D, H), v(1024, KK, dtype=F32), v(CH, 1, KK, dtype=F32), v(1024, KK), v(CH, 512, KK),
        v(512, KK, dtype=F32), v(512, KK), v(1, KK, dtype=F32),
        v(8, 64, KK), v(8, 1, KK, dtype=F32), v(64, KK), v(1, KK, dtype=F32),
        v(4, 64, KK), v(4, 1, KK, dtype=F32), v(8, 64, KK), v(512, KK), v(1024, 1024, dtype=F32),
        v(S, 4, R, D), v(S, 2, R, H), v(S, 2, R, D), v(S, R, D), v(S, 4, R, D),
        v(S, 4, R, D), v(S, 2, R, H), v(S, 2, R, D), v(4 * R, H), v(S, R, D), v(4, S, R, 512),
        sem(8), sem(1), sem(1), sem(2), sem(4), sem(1), sem(4), sem(4), sem(1), sem(1), sem(5), sem(5),
        sem(1), sem(S), sem(S), sem(1), sem(S), sem(S), sem(1), sem(S), sem(S), sem(1), sem(S), sem(1),
    ]
    return pl.pallas_call(
        kernel,
        out_shape=jax.ShapeDtypeStruct((1024, 512), BF16),
        in_specs=[any_space] * 15 + [vmem] * 2,
        out_specs=any_space,
        scratch_shapes=scratch,
        compiler_params=pltpu.CompilerParams(
            collective_id=0, has_side_effects=True, vmem_limit_bytes=67_000_000
        ),
    )(
        residual, query_wide, key_wide, value_wide, decay_wide, gate_wide, query_narrow, key_narrow,
        value_narrow, decay_narrow, gate_narrow, out_wide, out_narrow, up_weight, down_weight.T,
        head_gain.reshape(1, -1), mlp_gain.reshape(1, -1),
    )


def solution(mesh):
    return jax.shard_map(
        body,
        mesh=mesh,
        in_specs=(
            P("sp", None),
            *[P("sp", "tp")] * 10,
            P(),
            P("tp", None),
            P("tp", None),
            P(),
            P("sp", "tp"),
            P("tp", "sp"),
        ),
        out_specs=P("sp", "tp"),
        check_vma=False,
    )
```

time: 152 us -> 117 us (0.77)
  the two profiles are of different devices: /device:TPU:0 before, /device:TPU:1 now
where the time goes in v2:
time: 117 us
  Pallas kernels  114 us (97%)
  local copies, waits for them, and re-layouts  2.26 us (2%)
    pallas_call x1, Pallas kernels, body(): pl.pallas_call(kernel, out_shape=jax.ShapeDtypeStruct((1024, 512), BF16),...  114 us

profile of v2, /device:TPU:1, one launch (start us, length us, event | category | flops | bytes accessed | tf_op | source)
XLA Modules:
  0.0 116.6 jit_solution(17316126741770249737)
XLA Ops:
  0.0 114.3 %shard_map.163 = bf16[1024,512]{1,0:T(8,128)(2,1)} custom-call(bf16[1024,2048]{1,0:T(8,128)(2,1)} %res.1, bf16[1024,256]{1,0:T(8,128)(2,1)} %qw.1, bf16[1024,256]{1,0:T(8,128)(2,1)} %kw.1, bf16[1024,512]{1,0:T(8,128)(2,1)} %vw.1, bf16[1024,256]{1,0:T(8,128)(2,1)} %dw.1, bf16[1024,512]{1,0:T(8,128)(2,1)} %gw.1, bf16[1024,128]{1,0:T(8,128)(2,1)} %qn.1, ...), custom_call_target="tpu_custom_call" | custom-call | tf_op jit(solution)/shard_map/pallas_call | solution.py:540
  114.3 2.3 %copy.19 = bf16[1024,512]{1,0:T(8,128)(2,1)} copy(bf16[1024,512]{1,0:T(8,128)(2,1)} %shard_map.163) | data formatting | bytes 2097152
